TPU v7x, 32 devices: a whole 2x2x4 slice. The times are simulated.
32 devices in a mesh: fs: 4 (over z), rep: 4 (over y, x), tp: 2 (over core).
Axes of the slice: x: 2, y: 2, z: 4, core: 2. Of those that a mesh axis runs over, the one named last changes fastest.
Arguments:
- mixer_input: bfloat16 [32768, 2048], P(('fs', 'rep')), may hold values from -6 to 6
- value_cot: bfloat16 [32768, 2048], P(('fs', 'rep'), 'tp'), may hold values from -0.22097087 to 0.22097087
- gate_cot: bfloat16 [32768, 2048], P(('fs', 'rep'), 'tp'), may hold values from -0.22097087 to 0.22097087
- value_weight: float32 [2048, 2048], P('fs', 'tp'), may hold values from -0.125 to 0.125
- gate_weight: float32 [2048, 2048], P('fs', 'tp'), may hold values from -0.125 to 0.125
- value_basis: bfloat16 [2048, 256], replicated, may hold values from -0.8838835 to 0.8838835
- gate_basis: bfloat16 [2048, 256], replicated, may hold values from -0.8838835 to 0.8838835
- value_first: float32 [256, 2048], P('fs', 'tp'), may hold values from -6 to 6
- gate_first: float32 [256, 2048], P('fs', 'tp'), may hold values from -6 to 6
- value_second: float32 [256, 2048], P('fs', 'tp'), may hold values from 0.01 to 1
- gate_second: float32 [256, 2048], P('fs', 'tp'), may hold values from 0.01 to 1
Outputs:
- value_new: float32 [2048, 2048], P('fs', 'tp')
- gate_new: float32 [2048, 2048], P('fs', 'tp')
- value_copy: bfloat16 [2048, 2048], P(None, 'tp')
- gate_copy: bfloat16 [2048, 2048], P(None, 'tp')
- value_step: float32 [2048, 2048], P('fs', 'tp')
- gate_step: float32 [2048, 2048], P('fs', 'tp')
- value_first_new: float32 [256, 2048], P('fs', 'tp')
- gate_first_new: float32 [256, 2048], P('fs', 'tp')
- value_second_new: float32 [256, 2048], P('fs', 'tp')
- gate_second_new: float32 [256, 2048], P('fs', 'tp')
All inputs are finite; a program needn't handle non-finite values.
Results may differ from a plain program's by a relative error of at most 0.0044.
Values may be sent and summed in bfloat16 or wider, within the bound.
A program may use at most 128 MiB of HBM per device.

v0:
```python
import jax
import jax.numpy as jnp
from jax import lax
from jax.sharding import PartitionSpec as P

D = 2048
learn_rate = 0.02


def local(
    mixer_input,
    value_cot,
    gate_cot,
    value_weight,
    gate_weight,
    value_basis,
    gate_basis,
    value_first,
    gate_first,
    value_second,
    gate_second,
):
    half_cols = value_cot.shape[1]
    rows_dev = value_weight.shape[0]
    fs_index = lax.axis_index("fs")
    own_value = lax.dynamic_slice_in_dim(value_basis, fs_index * rows_dev, rows_dev, 0)
    own_gate = lax.dynamic_slice_in_dim(gate_basis, fs_index * rows_dev, rows_dev, 0)
    value_proj = jnp.dot(mixer_input, value_basis, preferred_element_type=jnp.float32)
    gate_proj = jnp.dot(mixer_input, gate_basis, preferred_element_type=jnp.float32)
    upper_value = lax.optimization_barrier(value_proj.astype(jnp.bfloat16))
    upper_gate = lax.optimization_barrier(gate_proj.astype(jnp.bfloat16))
    lower_value = (value_proj - upper_value.astype(jnp.float32)).astype(jnp.bfloat16)
    lower_gate = (gate_proj - upper_gate.astype(jnp.float32)).astype(jnp.bfloat16)
    value_part = jnp.dot(upper_value.T, value_cot, preferred_element_type=jnp.float32) + jnp.dot(
        lower_value.T, value_cot, preferred_element_type=jnp.float32
    )
    gate_part = jnp.dot(upper_gate.T, gate_cot, preferred_element_type=jnp.float32) + jnp.dot(
        lower_gate.T, gate_cot, preferred_element_type=jnp.float32
    )
    partial_value = lax.psum_scatter(
        jnp.concatenate([value_part, gate_part], axis=1), "fs", scatter_dimension=0, tiled=True
    )
    projected = lax.psum(partial_value, "rep")
    value_small = projected[:, :half_cols]
    gate_small = projected[:, half_cols:]
    value_first_new = 0.9 * value_first + 0.1 * value_small
    gate_first_new = 0.9 * gate_first + 0.1 * gate_small
    value_second_new = 0.95 * value_second + 0.05 * value_small * value_small
    gate_second_new = 0.95 * gate_second + 0.05 * gate_small * gate_small
    scaled = jnp.concatenate(
        [
            value_first_new * lax.rsqrt(value_second_new),
            gate_first_new * lax.rsqrt(gate_second_new),
        ],
        axis=1,
    ).astype(jnp.bfloat16)
    piece = lax.all_gather(scaled, "fs", axis=0, tiled=True)
    value_part = jnp.dot(own_value, piece[:, :half_cols], preferred_element_type=jnp.float32)
    gate_part = jnp.dot(own_gate, piece[:, half_cols:], preferred_element_type=jnp.float32)
    expanded = jnp.concatenate([value_part, gate_part], axis=1)
    value_full = expanded[:, :half_cols]
    gate_full = expanded[:, half_cols:]
    squares = lax.psum(
        (jnp.sum(value_full * value_full), jnp.sum(gate_full * gate_full)), ("fs", "tp")
    )
    entries = float(D * D)
    value_step = value_full * lax.rsqrt(squares[0] / entries + 1e-06)
    gate_step = gate_full * lax.rsqrt(squares[1] / entries + 1e-06)
    value_new = value_weight - learn_rate * value_step
    gate_new = gate_weight - learn_rate * gate_step
    copies = (
        lax.all_gather(value_new.astype(jnp.bfloat16), "fs", axis=0, tiled=True),
        lax.all_gather(gate_new.astype(jnp.bfloat16), "fs", axis=0, tiled=True),
    )
    return (
        value_new,
        gate_new,
        copies[0],
        copies[1],
        value_step,
        gate_step,
        value_first_new,
        gate_first_new,
        value_second_new,
        gate_second_new,
    )


def solution(mesh):
    return jax.shard_map(
        local,
        mesh=mesh,
        in_specs=(
            P(("fs", "rep"), None),
            P(("fs", "rep"), "tp"),
            P(("fs", "rep"), "tp"),
            P("fs", "tp"),
            P("fs", "tp"),
            P(),
            P(),
            P("fs", "tp"),
            P("fs", "tp"),
            P("fs", "tp"),
            P("fs", "tp"),
        ),
        out_specs=(
            P("fs", "tp"),
            P("fs", "tp"),
            P(None, "tp"),
            P(None, "tp"),
            P("fs", "tp"),
            P("fs", "tp"),
            P("fs", "tp"),
            P("fs", "tp"),
            P("fs", "tp"),
            P("fs", "tp"),
        ),
        check_vma=False,
    )
```

profile of v0, /device:TPU:0, one launch (start us, length us, event | category | flops | bytes accessed | tf_op | source)
XLA Modules:
  0.0 350.1 jit_solution(15234940572082400259)
XLA Ops:
  7.2 6.2 %fusion.15 = (bf16[2048,256]{1,0:T(8,128)(2,1)S(1)}, f32[2048,256]{1,0:T(8,128)S(1)}) fusion(bf16[2048,2048]{1,0:T(8,128)(2,1)} %param.11, bf16[2048,256]{1,0:T(8,128)(2,1)} %param.16), kind=kOutput, calls=%fused_computation.31 | convolution fusion | flops 2148007936 | bytes 12582912 | tf_op jit(solution)/shard_map/dot_general | solution.py:28
  13.5 0.1 copy-done.9
  13.6 2.4 fusion.14
  16.1 1.3 fusion.16
  17.3 1.3 convolution_add_fusion.1
  18.6 0.9 copy-done.2
  19.5 1.3 fusion.17
  20.8 1.3 convolution_add_fusion
  22.1 1.5 pad_maximum_fusion
  23.6 46.5 %reduce-scatter.2.cloned.1.call-done = f32[64,2048]{1,0:T(8,128)} async-done(((f32[256,2048]{1,0:T(8,128)}), f32[64,2048]{1,0:T(8,128)}) %reduce-scatter.2.cloned.1.call-update) | async-done | bytes 524304 | tf_op jit(solution)/shard_map/reduce_scatter | solution.py:40
  70.2 47.5 %all-reduce.3.cloned.1.call-done = f32[64,2048]{1,0:T(8,128)} async-done(((f32[64,2048]{1,0:T(8,128)}), f32[64,2048]{1,0:T(8,128)}) %all-reduce.3.cloned.1.call-update) | async-done | bytes 524304 | tf_op jit(solution)/shard_map/psum | solution.py:43
  117.7 2.1 multiply_convert_fusion.1
  119.8 0.7 pad_maximum_fusion.1
  120.5 0.0 all-gather.6.cloned.1.call-start
  120.6 28.1 %all-gather.4.cloned.1.call-done = bf16[256,2048]{1,0:T(8,128)(2,1)} async-done(((bf16[64,2048]{1,0:T(8,128)(2,1)}), bf16[256,2048]{1,0:T(8,128)(2,1)}) %all-gather.4.cloned.1.call-update) | async-done | bytes 1048592 | tf_op jit(solution)/shard_map/all_gather | solution.py:57
  148.7 2.4 multiply_reduce_fusion
  151.1 3.5 multiply_reduce_fusion.1
  154.6 15.3 %all-reduce = (f32[]{:T(128)}, f32[]{:T(128)}) all-reduce(f32[]{:T(128)} %get-tuple-element.31, f32[]{:T(128)} %get-tuple-element.33), channel_id=1, replica_groups=mesh['fs'=4,'rep'=4,'tp'=2] {'fs','tp'}, use_global_device_ids=true, to_apply=%region_3.0 | all-reduce | flops 2 | bytes 16 | tf_op jit(solution)/shard_map/psum | solution.py:63
  170.6 5.6 %fusion.11 = (bf16[512,1024]{1,0:T(8,128)(2,1)}, f32[512,1024]{1,0:T(8,128)}, f32[512,1024]{1,0:T(8,128)}) fusion(f32[512,1024]{1,0:T(8,128)} %param.14, f32[512,1024]{1,0:T(8,128)} %get-tuple-element.32, f32[]{:T(128)S(6)} %rsqrt.14), kind=kLoop, calls=%fused_computation.29 | loop fusion | flops 2097152 | bytes 9437188 | tf_op jit(solution)/shard_map/convert_element_type | solution.py:72
  177.0 4.8 %fusion.10 = (bf16[512,1024]{1,0:T(8,128)(2,1)}, f32[512,1024]{1,0:T(8,128)}, f32[512,1024]{1,0:T(8,128)}) fusion(f32[512,1024]{1,0:T(8,128)} %param.15, f32[512,1024]{1,0:T(8,128)S(1)} %get-tuple-element.34, f32[]{:T(128)S(6)} %rsqrt.15), kind=kLoop, calls=%fused_computation.28 | loop fusion | flops 2097152 | bytes 9437188 | tf_op jit(solution)/shard_map/convert_element_type | solution.py:73
  181.7 73.7 %all-gather.6.cloned.1.call-done = bf16[2048,1024]{1,0:T(8,128)(2,1)} async-done(((bf16[512,1024]{1,0:T(8,128)(2,1)}), bf16[2048,1024]{1,0:T(8,128)(2,1)}) %all-gather.6.cloned.1.call-update) | async-done | bytes 4194320 | tf_op jit(solution)/shard_map/all_gather | solution.py:72
  255.5 81.2 %all-gather.8.cloned.1.call-done = bf16[2048,1024]{1,0:T(8,128)(2,1)} async-done(((bf16[512,1024]{1,0:T(8,128)(2,1)}), bf16[2048,1024]{1,0:T(8,128)(2,1)}) %all-gather.8.cloned.1.call-update) | async-done | bytes 4194320 | tf_op jit(solution)/shard_map/all_gather | solution.py:73
  336.7 4.8 %copy.24 = bf16[2048,1024]{1,0:T(8,128)(2,1)} copy(bf16[2048,1024]{1,0:T(8,128)(2,1)} %all-gather.6.cloned.1.call-done) | data formatting | bytes 8388608
  341.5 2.0 copy.25
  (27 shorter events, 0.3 us)
Async XLA Ops:
  7.2 6.3 %copy-start = (bf16[2048,256]{1,0:T(8,128)(2,1)S(1)}, bf16[2048,256]{1,0:T(8,128)(2,1)}, u32[]{:S(2)}) copy-start(bf16[2048,256]{1,0:T(8,128)(2,1)} %param.17) | copy-start | bytes 3145732
  7.2 62.9 %reduce-scatter.2.cloned.1.call-start = ((), (), s32[]{:S(2)}) async-start(), calls=%async_computation.1 | async-start | bytes 2621440 | tf_op jit(solution)/shard_map/reduce_scatter | solution.py:40
  7.2 6.4 %copy-start.9 = (bf16[2048,2048]{1,0:T(8,128)(2,1)S(1)}, bf16[2048,2048]{1,0:T(8,128)(2,1)}, u32[]{:S(2)}) copy-start(bf16[2048,2048]{1,0:T(8,128)(2,1)} %param.11) | copy-start | bytes 25165828
  13.6 2.4 copy-start.1
  17.3 2.2 copy-start.2
  23.5 94.1 %copy-start.5 = (f32[64,1024]{1,0:T(8,128)S(1)}, f32[64,1024]{1,0:T(8,128)}, u32[]{:S(2)}) copy-start(f32[64,1024]{1,0:T(8,128)} %param.20) | copy-start | bytes 786436
  23.5 94.1 %copy-start.6 = (f32[64,1024]{1,0:T(8,128)S(1)}, f32[64,1024]{1,0:T(8,128)}, u32[]{:S(2)}) copy-start(f32[64,1024]{1,0:T(8,128)} %param.18) | copy-start | bytes 786436
  23.5 94.1 %copy-start.7 = (f32[64,1024]{1,0:T(8,128)S(1)}, f32[64,1024]{1,0:T(8,128)}, u32[]{:S(2)}) copy-start(f32[64,1024]{1,0:T(8,128)} %param.21) | copy-start | bytes 786436
  23.6 94.1 %copy-start.8 = (f32[64,1024]{1,0:T(8,128)S(1)}, f32[64,1024]{1,0:T(8,128)}, u32[]{:S(2)}) copy-start(f32[64,1024]{1,0:T(8,128)} %param.19) | copy-start | bytes 786436
  23.6 94.1 %all-reduce.3.cloned.1.call-start = ((), (), s32[]{:S(2)}) async-start(), calls=%async_computation.2 | async-start | bytes 1048576 | tf_op jit(solution)/shard_map/psum | solution.py:43
  70.1 78.6 %all-gather.4.cloned.1.call-start = ((), (), s32[]{:S(2)}) async-start(), calls=%async_computation.3 | async-start | bytes 1310720 | tf_op jit(solution)/shard_map/all_gather | solution.py:57
  120.5 134.9 %all-gather.6.cloned.1.call-start = ((), (), s32[]{:S(2)}) async-start(), calls=%async_computation.4 | async-start | bytes 5242880 | tf_op jit(solution)/shard_map/all_gather | solution.py:72
  148.7 2.4 copy-start.4
  176.2 160.5 %all-gather.8.cloned.1.call-start = ((), (), s32[]{:S(2)}) async-start(), calls=%async_computation.5 | async-start | bytes 5242880 | tf_op jit(solution)/shard_map/all_gather | solution.py:73
  336.7 4.8 %copy-start.3 = (bf16[2048,1024]{1,0:T(8,128)(2,1)S(1)}, bf16[2048,1024]{1,0:T(8,128)(2,1)}, u32[]{:S(2)}) copy-start(bf16[2048,1024]{1,0:T(8,128)(2,1)} %all-gather.8.cloned.1.call-done) | copy-start | bytes 12582916
Sparse Core Ops, SparseCore 0:
  23.7 46.3 reduce-scatter.1
  73.1 44.5 all-reduce.2
  120.7 27.9 all-gather.3
  176.3 79.0 all-gather.5
  257.5 79.2 all-gather.7
where the time goes:
time: 350 us
  waiting for transfers between devices  277 us (79%)
  matrix products  19.7 us (6%)
  blocking collectives  15.3 us (4%)
  between operations  15.3 us (4%)
  other arithmetic  14.6 us (4%)
  local copies, waits for them, and re-layouts  7.86 us (2%)
    all_gather x1, waiting for transfers between devices, local(): lax.all_gather(gate_new.astype(jnp.bfloat16), 'fs', axis=0, tiled=True)  81.2 us
    all_gather x1, waiting for transfers between devices, local(): lax.all_gather(value_new.astype(jnp.bfloat16), 'fs', axis=0, tiled=True)  73.7 us
    psum x1, waiting for transfers between devices, local(): projected = lax.psum(partial_value, 'rep')  47.5 us
    reduce_scatter x1, waiting for transfers between devices, local(): lax.psum_scatter(jnp.concatenate([value_part, gate_part], axis=1), 'fs',...  46.5 us
    all_gather x1, waiting for transfers between devices, local(): piece = lax.all_gather(scaled, 'fs', axis=0, tiled=True)  28.1 us
    psum x1, blocking collectives, local(): lax.psum((jnp.sum(value_full * value_full), jnp.sum(gate_full * gate_full...  15.3 us
    unnamed x22, local copies, waits for them, and re-layouts  7.86 us
  transfers between devices with their start and end apart: 5, of which 5 were waited for; matrix products, arithmetic and copies ran while one was open for 1% of the time, Pallas kernels for 0%

commit v1 on v0

--- a/solution.py
+++ b/solution.py
@@ -5,6 +5,11 @@
 
 D = 2048
 learn_rate = 0.02
+
+
+def summed_here(shard, axis):
+    blocks = lax.all_gather(shard, axis)
+    return jnp.sum(blocks, axis=0)
 
 
 def local(
@@ -40,7 +45,7 @@
     partial_value = lax.psum_scatter(
         jnp.concatenate([value_part, gate_part], axis=1), "fs", scatter_dimension=0, tiled=True
     )
-    projected = lax.psum(partial_value, "rep")
+    projected = summed_here(partial_value, "rep")
     value_small = projected[:, :half_cols]
     gate_small = projected[:, half_cols:]
     value_first_new = 0.9 * value_first + 0.1 * value_small

time: 350 us -> 340 us (0.971)
  waiting for transfers between devices: 277 us -> 266 us
    psum x1 -> x0, waiting for transfers between devices: 47.5 us -> none  [local(): projected = lax.psum(partial_value, 'rep')]
    all_gather x0 -> x1, waiting for transfers between devices: none -> 36.2 us  [summed_here(): blocks = lax.all_gather(shard, axis)]
where the time goes in v1:
time: 340 us; the launch traced here: 339 us
  waiting for transfers between devices  266 us (78%)
  matrix products  19.7 us (6%)
  other arithmetic  15.4 us (5%)
  blocking collectives  15.3 us (4%)
  between operations  15.3 us (4%)
  local copies, waits for them, and re-layouts  7.87 us (2%)
    all_gather x1, waiting for transfers between devices, local(): lax.all_gather(gate_new.astype(jnp.bfloat16), 'fs', axis=0, tiled=True)  81.2 us
    all_gather x1, waiting for transfers between devices, local(): lax.all_gather(value_new.astype(jnp.bfloat16), 'fs', axis=0, tiled=True)  73.7 us
    reduce_scatter x1, waiting for transfers between devices, local(): lax.psum_scatter(jnp.concatenate([value_part, gate_part], axis=1), 'fs',...  46.4 us
    all_gather x1, waiting for transfers between devices, summed_here(): blocks = lax.all_gather(shard, axis)  36.2 us
    all_gather x1, waiting for transfers between devices, local(): piece = lax.all_gather(scaled, 'fs', axis=0, tiled=True)  28.1 us
    psum x1, blocking collectives, local(): lax.psum((jnp.sum(value_full * value_full), jnp.sum(gate_full * gate_full...  15.3 us
    unnamed x22, local copies, waits for them, and re-layouts  7.87 us
  transfers between devices with their start and end apart: 5, of which 5 were waited for; matrix products, arithmetic and copies ran while one was open for 1% of the time, Pallas kernels for 0%

profile of v1, /device:TPU:0, one launch (start us, length us, event | category | flops | bytes accessed | tf_op | source)
XLA Modules:
  0.0 339.5 jit_solution(10073231918362812263)
XLA Ops:
  7.2 6.2 %fusion.15 = (bf16[2048,256]{1,0:T(8,128)(2,1)S(1)}, f32[2048,256]{1,0:T(8,128)S(1)}) fusion(bf16[2048,2048]{1,0:T(8,128)(2,1)} %param.11, bf16[2048,256]{1,0:T(8,128)(2,1)} %param.16), kind=kOutput, calls=%fused_computation.31 | convolution fusion | flops 2148007936 | bytes 12582912 | tf_op jit(solution)/shard_map/dot_general | solution.py:33
  13.5 0.1 copy-done.9
  13.6 2.4 fusion.14
  16.1 1.3 fusion.16
  17.3 1.3 convolution_add_fusion.1
  18.6 0.9 copy-done.2
  19.5 1.3 fusion.17
  20.8 1.3 convolution_add_fusion
  22.1 1.5 pad_maximum_fusion
  23.7 46.4 %reduce-scatter.2.cloned.1.call-done = f32[64,2048]{1,0:T(8,128)} async-done(((f32[256,2048]{1,0:T(8,128)}), f32[64,2048]{1,0:T(8,128)}) %reduce-scatter.2.cloned.1.call-update) | async-done | bytes 524304 | tf_op jit(solution)/shard_map/reduce_scatter | solution.py:45
  70.1 36.2 %all-gather.12.cloned.1.call-done = f32[256,2048]{1,0:T(8,128)} async-done(((f32[64,2048]{1,0:T(8,128)}), f32[256,2048]{1,0:T(8,128)}) %all-gather.12.cloned.1.call-update) | async-done | bytes 2097168 | tf_op jit(solution)/shard_map/all_gather | solution.py:11
  106.3 1.8 reduce_sum.27
  108.1 1.1 multiply_convert_fusion.1
  109.2 0.7 pad_maximum_fusion.1
  110.0 28.1 %all-gather.6.cloned.1.call-done = bf16[256,2048]{1,0:T(8,128)(2,1)} async-done(((bf16[64,2048]{1,0:T(8,128)(2,1)}), bf16[256,2048]{1,0:T(8,128)(2,1)}) %all-gather.6.cloned.1.call-update) | async-done | bytes 1048592 | tf_op jit(solution)/shard_map/all_gather | solution.py:62
  138.1 2.4 multiply_reduce_fusion
  140.5 3.5 %multiply_reduce_fusion.1 = (f32[]{:T(128)}, f32[512,1024]{1,0:T(8,128)}) fusion(bf16[256,2048]{1,0:T(8,128)(2,1)S(1)} %copy-done.4, bf16[2048,256]{1,0:T(8,128)(2,1)} %param.16, s32[]{:T(128)S(6)} %select_n.4), kind=kOutput, calls=%fused_computation.4 | convolution fusion | flops 269484032 | bytes 2883592 | tf_op jit(solution)/shard_map/dot_general | solution.py:63
  144.0 15.3 %all-reduce = (f32[]{:T(128)}, f32[]{:T(128)}) all-reduce(f32[]{:T(128)} %get-tuple-element.31, f32[]{:T(128)} %get-tuple-element.33), channel_id=1, replica_groups=mesh['fs'=4,'rep'=4,'tp'=2] {'fs','tp'}, use_global_device_ids=true, to_apply=%region_3.0 | all-reduce | flops 2 | bytes 16 | tf_op jit(solution)/shard_map/psum | solution.py:68
  160.0 5.6 %fusion.11 = (bf16[512,1024]{1,0:T(8,128)(2,1)}, f32[512,1024]{1,0:T(8,128)}, f32[512,1024]{1,0:T(8,128)}) fusion(f32[512,1024]{1,0:T(8,128)} %param.14, f32[512,1024]{1,0:T(8,128)} %get-tuple-element.32, f32[]{:T(128)S(6)} %rsqrt.14), kind=kLoop, calls=%fused_computation.29 | loop fusion | flops 2097152 | bytes 9437188 | tf_op jit(solution)/shard_map/convert_element_type | solution.py:77
  166.4 4.8 %fusion.10 = (bf16[512,1024]{1,0:T(8,128)(2,1)}, f32[512,1024]{1,0:T(8,128)}, f32[512,1024]{1,0:T(8,128)}) fusion(f32[512,1024]{1,0:T(8,128)} %param.15, f32[512,1024]{1,0:T(8,128)S(1)} %get-tuple-element.34, f32[]{:T(128)S(6)} %rsqrt.15), kind=kLoop, calls=%fused_computation.28 | loop fusion | flops 2097152 | bytes 9437188 | tf_op jit(solution)/shard_map/convert_element_type | solution.py:78
  171.1 73.7 %all-gather.8.cloned.1.call-done = bf16[2048,1024]{1,0:T(8,128)(2,1)} async-done(((bf16[512,1024]{1,0:T(8,128)(2,1)}), bf16[2048,1024]{1,0:T(8,128)(2,1)}) %all-gather.8.cloned.1.call-update) | async-done | bytes 4194320 | tf_op jit(solution)/shard_map/all_gather | solution.py:77
  244.9 81.2 %all-gather.10.cloned.1.call-done = bf16[2048,1024]{1,0:T(8,128)(2,1)} async-done(((bf16[512,1024]{1,0:T(8,128)(2,1)}), bf16[2048,1024]{1,0:T(8,128)(2,1)}) %all-gather.10.cloned.1.call-update) | async-done | bytes 4194320 | tf_op jit(solution)/shard_map/all_gather | solution.py:78
  326.1 4.8 %copy.23 = bf16[2048,1024]{1,0:T(8,128)(2,1)} copy(bf16[2048,1024]{1,0:T(8,128)(2,1)} %all-gather.8.cloned.1.call-done) | data formatting | bytes 8388608
  330.9 2.0 copy.24
  (28 shorter events, 0.3 us)
Async XLA Ops:
  7.2 6.3 %copy-start = (bf16[2048,256]{1,0:T(8,128)(2,1)S(1)}, bf16[2048,256]{1,0:T(8,128)(2,1)}, u32[]{:S(2)}) copy-start(bf16[2048,256]{1,0:T(8,128)(2,1)} %param.17) | copy-start | bytes 3145732
  7.2 62.9 %reduce-scatter.2.cloned.1.call-start = ((), (), s32[]{:S(2)}) async-start(), calls=%async_computation.1 | async-start | bytes 2621440 | tf_op jit(solution)/shard_map/reduce_scatter | solution.py:45
  7.2 6.4 %copy-start.9 = (bf16[2048,2048]{1,0:T(8,128)(2,1)S(1)}, bf16[2048,2048]{1,0:T(8,128)(2,1)}, u32[]{:S(2)}) copy-start(bf16[2048,2048]{1,0:T(8,128)(2,1)} %param.11) | copy-start | bytes 25165828
  13.6 2.4 copy-start.1
  17.3 2.2 copy-start.2
  23.6 84.5 %copy-start.5 = (f32[64,1024]{1,0:T(8,128)S(1)}, f32[64,1024]{1,0:T(8,128)}, u32[]{:S(2)}) copy-start(f32[64,1024]{1,0:T(8,128)} %param.20) | copy-start | bytes 786436
  23.6 84.5 %copy-start.6 = (f32[64,1024]{1,0:T(8,128)S(1)}, f32[64,1024]{1,0:T(8,128)}, u32[]{:S(2)}) copy-start(f32[64,1024]{1,0:T(8,128)} %param.18) | copy-start | bytes 786436
  23.6 84.5 %copy-start.7 = (f32[64,1024]{1,0:T(8,128)S(1)}, f32[64,1024]{1,0:T(8,128)}, u32[]{:S(2)}) copy-start(f32[64,1024]{1,0:T(8,128)} %param.21) | copy-start | bytes 786436
  23.6 84.5 %copy-start.8 = (f32[64,1024]{1,0:T(8,128)S(1)}, f32[64,1024]{1,0:T(8,128)}, u32[]{:S(2)}) copy-start(f32[64,1024]{1,0:T(8,128)} %param.19) | copy-start | bytes 786436
  23.6 82.7 %all-gather.12.cloned.1.call-start = ((), (), s32[]{:S(2)}) async-start(), calls=%async_computation.5 | async-start | bytes 2621440 | tf_op jit(solution)/shard_map/all_gather | solution.py:11
  70.1 68.0 %all-gather.6.cloned.1.call-start = ((), (), s32[]{:S(2)}) async-start(), calls=%async_computation.2 | async-start | bytes 1310720 | tf_op jit(solution)/shard_map/all_gather | solution.py:62
  110.0 134.9 %all-gather.8.cloned.1.call-start = ((), (), s32[]{:S(2)}) async-start(), calls=%async_computation.3 | async-start | bytes 5242880 | tf_op jit(solution)/shard_map/all_gather | solution.py:77
  138.1 2.4 copy-start.4
  165.6 160.5 %all-gather.10.cloned.1.call-start = ((), (), s32[]{:S(2)}) async-start(), calls=%async_computation.4 | async-start | bytes 5242880 | tf_op jit(solution)/shard_map/all_gather | solution.py:78
  326.1 4.8 %copy-start.3 = (bf16[2048,1024]{1,0:T(8,128)(2,1)S(1)}, bf16[2048,1024]{1,0:T(8,128)(2,1)}, u32[]{:S(2)}) copy-start(bf16[2048,1024]{1,0:T(8,128)(2,1)} %all-gather.10.cloned.1.call-done) | copy-start | bytes 12582916
Sparse Core Ops, SparseCore 0:
  23.7 46.3 reduce-scatter.1
  71.9 34.3 all-gather.11
  110.1 27.9 all-gather.5
  165.7 79.0 all-gather.7
  246.9 79.2 all-gather.9
